TPU v7x, 256 devices: a whole 4x4x8 slice. The times are simulated.
256 devices in a mesh: ep: 64 (over z, x, core), tp: 4 (over y).
Axes of the slice: x: 4, y: 4, z: 8, core: 2. Of those that a mesh axis runs over, the one named last changes fastest.
Arguments:
- mixer_input: bfloat16 [32768, 2048], P('ep'), may hold values from -6 to 6
- mixer_gain: float32 [2048], replicated, may hold values from 0.1 to 1.9
- query_weight: bfloat16 [2048, 1024], P(None, 'tp'), may hold values from -0.125 to 0.125
- key_weight: bfloat16 [2048, 1024], P(None, 'tp'), may hold values from -0.125 to 0.125
- value_weight: bfloat16 [2048, 1024], P(None, 'tp'), may hold values from -0.125 to 0.125
- gate_weight: bfloat16 [2048, 1024], P(None, 'tp'), may hold values from -0.125 to 0.125
- head_gain: float32 [1024], P('tp'), may hold values from 0.1 to 1.9
- output_weight: bfloat16 [1024, 2048], P('tp'), may hold values from -0.1875 to 0.1875
- log_decay: float32 [32768, 8], P('ep', 'tp'), may hold values from -1 to 0, as said below
- expert_input: bfloat16 [32768, 2048], P(('ep', 'tp')), may hold values from -6 to 6
- expert_gain: float32 [2048], replicated, may hold values from 0.1 to 1.9
- routes: int32 [32768, 2], P(('ep', 'tp')), may hold values from 0 to 63, all different within a row; in each aligned block of 128 rows (0 to 127, 128 to 255, ...) at most 6 rows name the same one
- route_weight: float32 [32768, 2], P(('ep', 'tp')), may hold values from 0.1 to 1
- expert_gate: bfloat16 [64, 2048, 1024], P('ep', None, 'tp'), may hold values from -0.125 to 0.125
- expert_up: bfloat16 [64, 2048, 1024], P('ep', None, 'tp'), may hold values from -0.125 to 0.125
- expert_down: bfloat16 [64, 1024, 2048], P('ep', 'tp'), may hold values from -0.1875 to 0.1875
Outputs:
- mixer_output: bfloat16 [32768, 2048], P(('ep', 'tp'))
- expert_output: bfloat16 [32768, 2048], P(('ep', 'tp'))
Inputs may be any that keep to these rules, and one draw needn't show every extreme that they name: `routes`: each row names 2 different experts. Among the rows of one device no expert is named more than 6 times, and in every draw the rows of some device name some expert exactly 6 times. `log_decay`: negative values.
All inputs are finite; a program needn't handle non-finite values.
Results may differ from a plain program's by a relative error of at most 0.025.
Values may be sent and summed in bfloat16 or wider, within the bound.
A program may use at most 128 MiB of HBM per device.

v0:
```python
import jax
import jax.numpy as jnp
from jax import lax
from jax.sharding import Mesh
from jax.sharding import PartitionSpec as P

BLOCK = 128
EP = ("ep_0", "ep_1", "ep_2")
EP_TP = ("ep_0", "ep_1", "ep_2", "tp")
EPS = 1e-06


def filled_with(x, identity):
    return jax.tree.map(
        lambda part, zero: jnp.zeros_like(part) + jnp.asarray(zero, part.dtype), x, identity
    )


def carried_in(x, axes, combine, identity):
    before = start = filled_with(x, identity)
    running = x
    for axis in reversed(axes):
        peers, position = (lax.axis_size(axis), lax.axis_index(axis))
        pieces = jax.tree.map(
            lambda part, kind: lax.all_gather(part.astype(kind), axis),
            running,
            (jnp.bfloat16, jnp.bfloat16),
        )
        inside, running = (start, start)
        for k in range(peers):
            passed = k < position
            running = combine(
                running, jax.tree.map(lambda part, own: part[k].astype(own.dtype), pieces, x)
            )
            inside = jax.tree.map(lambda new, old: jnp.where(passed, new, old), running, inside)
        before = combine(inside, before)
    return before


def norm_rows(values, gain):
    floats = values.astype(jnp.float32)
    scale = lax.rsqrt(jnp.mean(floats * floats, axis=-1, keepdims=True) + EPS)
    return (floats * scale * gain).astype(jnp.bfloat16)


def rotate(values, position):
    half_dim = values.shape[-1] // 2
    frequency = 10000.0 ** (-jnp.arange(half_dim, dtype=jnp.float32) / half_dim)
    angles = position.astype(jnp.float32)[:, None] * frequency[None, :]
    cosine = jnp.cos(angles)[:, None, :]
    sine_part = jnp.sin(angles)[:, None, :]
    first_half = values[..., :half_dim]
    second = values[..., half_dim:]
    return jnp.concatenate(
        [first_half * cosine - second * sine_part, first_half * sine_part + second * cosine],
        axis=-1,
    )


def chain_pair(earlier, following):
    return (earlier[0] * following[0], following[0][:, None, None] * earlier[1] + following[1])


def mixer_half(
    mixer_input,
    mixer_gain,
    query_weight,
    key_weight,
    value_weight,
    gate_weight,
    head_gain,
    output_weight,
    log_decay,
):
    row_count = mixer_input.shape[0]
    head_count = log_decay.shape[1]
    mix_width = query_weight.shape[1]
    head_dim = mix_width // head_count
    normed = norm_rows(mixer_input, mixer_gain)

    def project(weight):
        return jnp.dot(normed, weight, preferred_element_type=jnp.float32).astype(jnp.bfloat16)

    queries = project(query_weight)
    keys_raw = project(key_weight)
    values_new = project(value_weight)
    gate_raw = project(gate_weight)
    position = lax.axis_index(EP) * row_count + jnp.arange(row_count, dtype=jnp.int32)
    q_rot = rotate(
        queries.astype(jnp.float32).reshape(row_count, head_count, head_dim), position
    ).astype(jnp.bfloat16)
    k_rot = (
        rotate(keys_raw.astype(jnp.float32).reshape(row_count, head_count, head_dim), position)
        * head_dim ** (-0.5)
    ).astype(jnp.bfloat16)
    block_count = row_count // BLOCK
    q_blocks = q_rot.reshape(block_count, BLOCK, head_count, head_dim)
    k_blocks = k_rot.reshape(block_count, BLOCK, head_count, head_dim)
    v_blocks = values_new.reshape(block_count, BLOCK, head_count, head_dim)
    log_steps = log_decay.reshape(block_count, BLOCK, head_count)
    row_ids = lax.broadcasted_iota(jnp.int32, (BLOCK, BLOCK), 0)
    col_ids = lax.broadcasted_iota(jnp.int32, (BLOCK, BLOCK), 1)
    lower_mask = col_ids <= row_ids
    cumulative = jnp.einsum("ij,bjh->bhi", lower_mask.astype(jnp.float32), log_steps)
    block_total = cumulative[:, :, -1]
    differences = cumulative[:, :, :, None] - cumulative[:, :, None, :]
    decays = jnp.where(lower_mask, jnp.exp(jnp.where(lower_mask, differences, 0.0)), 0.0)
    scores = jnp.einsum("bihd,bjhd->bhij", q_blocks, k_blocks, preferred_element_type=jnp.float32)
    weights = (scores * decays).astype(jnp.bfloat16)
    inner_term = jnp.einsum(
        "bhij,bjhe->bihe", weights, v_blocks, preferred_element_type=jnp.float32
    )
    key_scale = jnp.exp(block_total[:, :, None] - cumulative)
    updates = jnp.einsum(
        "bhj,bjhd,bjhe->bhde", key_scale, k_blocks.astype(jnp.float32), v_blocks.astype(jnp.float32)
    )
    factor = jnp.exp(block_total)
    local_state = jnp.zeros((head_count, head_dim, head_dim), jnp.float32)
    for block_index in range(block_count):
        local_state = factor[block_index][:, None, None] * local_state + updates[block_index]
    entering = carried_in(
        (jnp.exp(jnp.sum(block_total, axis=0)), local_state),
        EP,
        chain_pair,
        (jnp.ones((head_count,), jnp.float32), jnp.zeros_like(local_state)),
    )
    carry_state = entering[1]
    starts = []
    for block_index in range(block_count):
        starts.append(carry_state)
        carry_state = factor[block_index][:, None, None] * carry_state + updates[block_index]
    carried = jnp.stack(starts)
    cross_term = jnp.einsum(
        "bhi,bihd,bhde->bihe", jnp.exp(cumulative), q_blocks.astype(jnp.float32), carried
    )
    retained = (inner_term + cross_term).reshape(row_count, head_count, head_dim)
    centre = jnp.mean(retained, axis=-1, keepdims=True)
    spread = jnp.mean(jnp.square(retained - centre), axis=-1, keepdims=True)
    scaled = (retained - centre) * lax.rsqrt(spread + EPS) * head_gain.reshape(head_count, head_dim)
    mixer_hidden = (
        scaled.reshape(row_count, mix_width) * jax.nn.silu(gate_raw.astype(jnp.float32))
    ).astype(jnp.bfloat16)
    return lax.psum_scatter(
        jnp.dot(mixer_hidden, output_weight, preferred_element_type=jnp.float32).astype(
            jnp.bfloat16
        ),
        "tp",
        scatter_dimension=0,
        tiled=True,
    )


def expert_half(
    expert_input, expert_gain, routes, route_weight, expert_gate, expert_up, expert_down
):
    tok_count, top_count = routes.shape
    experts = lax.axis_size(EP)
    capacity = max(2, 3 * tok_count * top_count // (2 * experts))
    width = expert_input.shape[1]
    normed = norm_rows(expert_input, expert_gain)
    flat_routes = routes.reshape(-1)
    entries = flat_routes.shape[0]
    onehot = (flat_routes[:, None] == jnp.arange(experts, dtype=jnp.int32)[None, :]).astype(
        jnp.bfloat16
    )
    before = (
        lax.broadcasted_iota(jnp.int32, (entries, entries), 1)
        < lax.broadcasted_iota(jnp.int32, (entries, entries), 0)
    ).astype(jnp.bfloat16)
    prior_count = jnp.dot(before, onehot, preferred_element_type=jnp.float32)
    slot_index = jnp.sum(prior_count * onehot.astype(jnp.float32), axis=1).astype(jnp.int32)
    target = flat_routes * capacity + slot_index
    token_ids = jnp.arange(entries, dtype=jnp.int32) // top_count
    slot_table = jnp.full((experts * capacity,), tok_count, jnp.int32).at[target].set(token_ids)
    padded = jnp.concatenate([normed, jnp.zeros((1, width), jnp.bfloat16)], axis=0)
    outgoing = jnp.take(padded, slot_table, axis=0).reshape(experts, capacity, width)
    arrived = lax.all_to_all(outgoing, EP, split_axis=0, concat_axis=0, tiled=True)
    sources = arrived.shape[0]
    flat_rows = arrived.reshape(sources * capacity, width)
    shard_piece = lax.all_gather((expert_gate[0], expert_up[0]), "tp", axis=1, tiled=True)
    gate_part = jnp.dot(flat_rows, shard_piece[0], preferred_element_type=jnp.float32)
    up_part = jnp.dot(flat_rows, shard_piece[1], preferred_element_type=jnp.float32)
    hidden = (jax.nn.silu(gate_part) * up_part).astype(jnp.bfloat16)
    reduced = jnp.dot(
        hidden,
        lax.all_gather(expert_down[0], "tp", axis=0, tiled=True),
        preferred_element_type=jnp.float32,
    )
    results = reduced.astype(jnp.bfloat16).reshape(sources, capacity, width)
    returned = lax.all_to_all(results, EP, split_axis=0, concat_axis=0, tiled=True)
    picked = jnp.take(returned.reshape(experts * capacity, width), target, axis=0)
    picked = picked.astype(jnp.float32).reshape(tok_count, top_count, width)
    norm_weight = route_weight / jnp.sum(route_weight, axis=1, keepdims=True)
    return jnp.sum(picked * norm_weight[:, :, None], axis=1).astype(jnp.bfloat16)


def on_device(
    mixer_input,
    mixer_gain,
    query_weight,
    key_weight,
    value_weight,
    gate_weight,
    head_gain,
    output_weight,
    log_decay,
    expert_input,
    expert_gain,
    routes,
    route_weight,
    expert_gate,
    expert_up,
    expert_down,
):
    mixer_output = mixer_half(
        mixer_input,
        mixer_gain,
        query_weight,
        key_weight,
        value_weight,
        gate_weight,
        head_gain,
        output_weight,
        log_decay,
    )
    expert_output = expert_half(
        expert_input, expert_gain, routes, route_weight, expert_gate, expert_up, expert_down
    )
    return (mixer_output, expert_output)


def solution(mesh):
    finer = Mesh(mesh.devices.reshape(8, 4, 2, mesh.shape["tp"]), ("ep_0", "ep_1", "ep_2", "tp"))
    placed = (
        P(EP, None),
        P(),
        P(None, "tp"),
        P(None, "tp"),
        P(None, "tp"),
        P(None, "tp"),
        P("tp"),
        P("tp", None),
        P(EP, "tp"),
        P(EP_TP, None),
        P(),
        P(EP_TP, None),
        P(EP_TP, None),
        P(EP, None, "tp"),
        P(EP, None, "tp"),
        P(EP, "tp", None),
    )
    return jax.shard_map(
        on_device,
        mesh=finer,
        in_specs=placed,
        out_specs=(P(EP_TP, None), P(EP_TP, None)),
        check_vma=False,
    )
```

profile of v0, /device:TPU:2, one launch (start us, length us, event | category | flops | bytes accessed | tf_op | source)
XLA Modules:
  0.0 269.4 jit_solution(11428957834506784839)
XLA Ops:
  11.4 3.1 %gather_fusion = bf16[384,2048]{1,0:T(8,128)(2,1)} fusion(bf16[129,2048]{1,0:T(8,128)(2,1)S(1)} %concatenate.26, s32[1024]{0:T(1024)S(1)} %pad_clamp_fusion.1), kind=kCustom, calls=%fused_computation | custom fusion | bytes 3147264 | tf_op jit(solution)/shard_map/jit(_take)/gather | solution.py:176
  14.5 2.5 gather.13
  17.2 1.6 broadcast_select_fusion
  18.8 12.0 %all-to-all-start = ((bf16[64,6,2048]{2,1,0:T(8,128)(2,1)}), bf16[64,6,2048]{2,1,0:T(8,128)(2,1)S(1)}, u32[]{:S(2)}, u32[]{:S(2)}) async-start(bf16[64,6,2048]{2,1,0:T(8,128)(2,1)} %broadcast_select_fusion), calls=%async_computation.1 | async-start | bytes 4194304 | tf_op jit(solution)/shard_map/all_to_all | solution.py:177
  31.7 2.1 fusion
  35.4 2.8 %convolution_convert_fusion.3 = bf16[512,256]{0,1:T(8,128)(2,1)S(1)} fusion(bf16[2048,256]{1,0:T(8,128)(2,1)} %param.18, bf16[512,2048]{1,0:T(8,128)(2,1)} %param.16, f32[2048]{0:T(1024)S(1)} %copy-done.25, f32[512]{0:T(512)S(1)} %add_rsqrt_fusion), kind=kOutput, calls=%fused_computation.28 | convolution fusion | flops 541196288 | bytes 3418112 | tf_op jit(solution)/shard_map/dot_general | solution.py:82
  38.4 3.5 %convolution_convert_fusion.2 = bf16[512,256]{0,1:T(8,128)(2,1)} fusion(bf16[2048,256]{1,0:T(8,128)(2,1)} %param.19, bf16[512,2048]{1,0:T(8,128)(2,1)} %param.16, f32[2048]{0:T(1024)S(1)} %copy-done.25, f32[512]{0:T(512)S(1)} %add_rsqrt_fusion), kind=kOutput, calls=%fused_computation.27 | convolution fusion | flops 541196288 | bytes 3418112 | tf_op jit(solution)/shard_map/dot_general | solution.py:82
  41.9 2.4 all-reduce.1
  44.9 7.8 %all-gather.4 = bf16[4,1,2]{2,1,0:T(2,128)(2,1)S(1)} all-gather(bf16[1,1,2]{2,1,0:T(2,128)(2,1)S(1)} %convert_bitcast_fusion), channel_id=1, replica_groups=mesh['ep_0'=8,'ep_1'=4,'ep_2'=2,'tp'=4] {'ep_1'}, dimensions={0}, use_global_device_ids=true | all-gather | bytes 20 | tf_op jit(solution)/shard_map/all_gather | solution.py:25
  53.6 1.8 convert.28
  55.9 2.3 subtract_convert_fusion
  62.4 2.6 convolution_convert_fusion.4
  69.8 1.9 all_gather.36
  75.1 16.2 %all-gather.5 = bf16[8,1,2]{2,1,0:T(2,128)(2,1)S(1)} all-gather(bf16[1,1,2]{2,1,0:T(2,128)(2,1)S(1)} %fusion.73), channel_id=1, replica_groups=mesh['ep_0'=8,'ep_1'=4,'ep_2'=2,'tp'=4] {'ep_0'}, dimensions={0}, use_global_device_ids=true | all-gather | bytes 36 | tf_op jit(solution)/shard_map/all_gather | solution.py:25
  93.5 1.8 copy.59
  96.9 1.8 copy.60
  98.6 12.1 %all_gather.37 = bf16[4,2,128,128]{3,2,1,0:T(8,128)(2,1)S(1)} all-gather(bf16[1,2,128,128]{3,2,1,0:T(8,128)(2,1)} %fusion.56), channel_id=1, replica_groups=mesh['ep_0'=8,'ep_1'=4,'ep_2'=2,'tp'=4] {'ep_1'}, dimensions={0}, use_global_device_ids=true | all-gather | bytes 327680 | tf_op jit(solution)/shard_map/all_gather | solution.py:25
  111.5 25.7 %all_gather.38 = bf16[8,2,128,128]{3,2,1,0:T(8,128)(2,1)S(1)} all-gather(bf16[1,2,128,128]{3,2,1,0:T(8,128)(2,1)S(1)} %fusion.55), channel_id=1, replica_groups=mesh['ep_0'=8,'ep_1'=4,'ep_2'=2,'tp'=4] {'ep_0'}, dimensions={0}, use_global_device_ids=true | all-gather | bytes 589824 | tf_op jit(solution)/shard_map/all_gather | solution.py:25
  140.1 2.8 %fusion.90 = (f32[4,128,2]{1,2,0:T(2,128)S(1)}, f32[4,128,2,128]{1,3,2,0:T(8,128)}) fusion(f32[4,128,2,128]{1,3,2,0:T(8,128)} %convolution_bitcast_fusion.1, bf16[4,128,2,128]{3,1,2,0:T(8,128)(2,1)S(1)} %fusion.27, f32[4,2,128]{2,1,0:T(2,128)S(1)} %copy-done.18, pred[128,128]{1,0:T(8,128)(4,1)} %iota_compare_fusion.4, bf16[4,128,2,64]{3,1,2,0:T(8,128)(2,1)} %copy.60, ...), kind=kOutput, calls=%fused_computation.178 | convolution fusion | flops 68549632 | bytes 1859584 | tf_op jit(solution)/shard_map/bhij,bjhe->bihe/dot_general | solution.py:110
  142.9 2.1 copy.71
  148.6 2.3 sub.60
  150.9 6.0 %convolution_convert_fusion = bf16[512,2048]{1,0:T(8,128)(2,1)} fusion(bf16[256,2048]{1,0:T(8,128)(2,1)S(1)} %copy-done, f32[64,8,2,128]{3,2,1,0:T(2,128)} %bitcast.151, f32[64,8,2,128]{3,2,1,0:T(2,128)} %bitcast.152, f32[64,8,2,128]{3,2,1,0:T(2,128)} %bitcast.153, bf16[2048,256]{1,0:T(8,128)(2,1)} %param.21, f32[256]{0:T(256)S(1)} %copy-done.27, ...), kind=kOutput, calls=%fused_computation.14 | convolution fusion | flops 1080426496 | bytes 7875584 | tf_op jit(solution)/shard_map/dot_general | solution.py:144
  158.4 5.8 %fusion.7 = f32[384,1024]{1,0:T(8,128)} fusion(bf16[384,2048]{1,0:T(8,128)(2,1)} %reshape.379, bf16[1,2048,1024]{2,1,0:T(8,128)(2,1)} %all-gather.10.cloned.1.call-done), kind=kOutput, calls=%fused_computation.12 | convolution fusion | flops 1610612736 | bytes 7340032 | tf_op jit(solution)/shard_map/dot_general | solution.py:181
  164.2 12.8 %all-gather.14.cloned.1.call-done = bf16[1,1024,2048]{2,1,0:T(8,128)(2,1)} async-done(((bf16[1,256,2048]{2,1,0:T(8,128)(2,1)}), bf16[1,1024,2048]{2,1,0:T(8,128)(2,1)}) %all-gather.14.cloned.1.call-update) | async-done | bytes 4194320 | tf_op jit(solution)/shard_map/all_gather | solution.py:186
  177.0 8.6 %fusion.9 = bf16[384,2048]{1,0:T(8,128)(2,1)} fusion(bf16[1,1024,2048]{2,1,0:T(8,128)(2,1)} %all-gather.14.cloned.1.call-done, f32[384,1024]{1,0:T(8,128)} %fusion.7, bf16[384,2048]{1,0:T(8,128)(2,1)S(1)} %copy-done.3, bf16[1,2048,1024]{2,1,0:T(8,128)(2,1)} %all-gather.12.cloned.1.call-done), kind=kOutput, calls=%fused_computation.15 | convolution fusion | flops 3224371200 | bytes 13107200 | tf_op jit(solution)/shard_map/dot_general | solution.py:184
  185.6 3.7 %reshape.380 = bf16[64,6,2048]{2,1,0:T(8,128)(2,1)} reshape(bf16[384,2048]{1,0:T(8,128)(2,1)} %fusion.9) | data formatting | bytes 3145728 | tf_op jit(solution)/shard_map/reshape | solution.py:189
  189.3 10.9 %all-to-all-start.1 = ((bf16[64,6,2048]{2,1,0:T(8,128)(2,1)}), bf16[64,6,2048]{2,1,0:T(8,128)(2,1)}, u32[]{:S(2)}, u32[]{:S(2)}) async-start(bf16[64,6,2048]{2,1,0:T(8,128)(2,1)} %reshape.380), calls=%async_computation.2 | async-start | bytes 4194304 | tf_op jit(solution)/shard_map/all_to_all | solution.py:190
  200.7 50.6 %all-to-all-done.1 = bf16[64,6,2048]{2,1,0:T(8,128)(2,1)} async-done(((bf16[64,6,2048]{2,1,0:T(8,128)(2,1)}), bf16[64,6,2048]{2,1,0:T(8,128)(2,1)}, u32[]{:S(2)}, u32[]{:S(2)}) %all-to-all-start.1) | async-done | bytes 1572896 | tf_op jit(solution)/shard_map/all_to_all | solution.py:190
  251.3 2.6 reshape.381
  253.9 2.3 gather_fusion.1
  256.2 1.7 gather.15
  258.0 4.9 %multiply_reduce_fusion = bf16[128,2048]{1,0:T(8,128)(2,1)} fusion(bf16[128,2,2048]{2,1,0:T(2,128)(2,1)S(1)} %gather.15, pred[128,2]{1,0:T(8,128)(4,1)S(1)} %copy.76, f32[128,2]{1,0:T(8,128)S(1)} %copy.78), kind=kLoop, calls=%fused_computation.16 | loop fusion | flops 1835008 | bytes 1574144 | tf_op jit(solution)/shard_map/reduce_sum | solution.py:194
  (144 shorter events, 33.3 us)
Async XLA Ops:
  7.2 143.8 %copy-start = (bf16[256,2048]{1,0:T(8,128)(2,1)S(1)}, bf16[256,2048]{1,0:T(8,128)(2,1)}, u32[]{:S(2)}) copy-start(bf16[256,2048]{1,0:T(8,128)(2,1)} %param.23) | copy-start | bytes 3145732
  7.2 1.5 copy-start.8
  7.2 2.3 copy-start.2
  7.2 2.5 copy-start.10
  7.2 151.2 %all-gather.10.cloned.1.call-start = ((), (), s32[]{:S(2)}) async-start(), calls=%async_computation.4 | async-start | bytes 5242880 | tf_op jit(solution)/shard_map/all_gather | solution.py:180
  7.9 156.3 %all-gather.12.cloned.1.call-start = ((), (), s32[]{:S(2)}) async-start(), calls=%async_computation.5 | async-start | bytes 5242880 | tf_op jit(solution)/shard_map/all_gather | solution.py:180
  9.2 2.2 copy-start.6
  9.9 1.4 copy-start.15
  18.8 138.2 %all-to-all-start = ((bf16[64,6,2048]{2,1,0:T(8,128)(2,1)}), bf16[64,6,2048]{2,1,0:T(8,128)(2,1)S(1)}, u32[]{:S(2)}, u32[]{:S(2)}) async-start(bf16[64,6,2048]{2,1,0:T(8,128)(2,1)} %broadcast_select_fusion), calls=%async_computation.1 | async-start | bytes 4194304 | tf_op jit(solution)/shard_map/all_to_all | solution.py:177
  30.8 2.9 %copy-start.17 = (f32[512,2]{0,1:T(2,128)S(1)}, f32[512,2]{0,1:T(2,128)}, u32[]{:S(2)}) copy-start(f32[512,2]{0,1:T(2,128)} %param.24) | copy-start | bytes 12292
  30.9 3.3 %copy-start.28 = (u32[256]{0:T(256)S(1)}, u32[256]{0:T(256)}, u32[]{:S(2)}) copy-start(u32[256]{0:T(256)} %constant.123) | copy-start | bytes 3076
  30.9 4.5 %copy-start.25 = (f32[2048]{0:T(1024)S(1)}, f32[2048]{0:T(1024)}, u32[]{:S(2)}) copy-start(f32[2048]{0:T(1024)} %param.17) | copy-start | bytes 24580
  30.9 146.1 %all-gather.14.cloned.1.call-start = ((), (), s32[]{:S(2)}) async-start(), calls=%async_computation.6 | async-start | bytes 5242880 | tf_op jit(solution)/shard_map/all_gather | solution.py:186
  31.6 231.3 %reduce-scatter.2.cloned.1.call-start = ((), (), s32[]{:S(2)}) async-start(), calls=%async_computation.3 | async-start | bytes 2621440 | tf_op jit(solution)/shard_map/reduce_scatter | solution.py:143
  33.8 28.6 %copy-start.22 = (f32[512]{0:T(512)}, f32[512]{0:T(512)S(1)}, u32[]{:S(2)}) copy-start(f32[512]{0:T(512)S(1)} %add_rsqrt_fusion) | copy-start | bytes 6148
  66.0 2.9 %copy-start.11 = (f32[2]{0:T(128)}, f32[2]{0:T(128)S(1)}, u32[]{:S(2)}) copy-start(f32[2]{0:T(128)S(1)} %get-tuple-element.6) | copy-start | bytes 28
  66.0 2.9 %copy-start.13 = (f32[2]{0:T(128)}, f32[2]{0:T(128)S(1)}, u32[]{:S(2)}) copy-start(f32[2]{0:T(128)S(1)} %get-tuple-element.7) | copy-start | bytes 28
  66.1 2.9 %copy-start.21 = (f32[2]{0:T(128)}, f32[2]{0:T(128)S(1)}, u32[]{:S(2)}) copy-start(f32[2]{0:T(128)S(1)} %get-tuple-element.5) | copy-start | bytes 28
  72.4 2.7 %copy-start.20 = (f32[2]{0:T(128)}, f32[2]{0:T(128)S(1)}, u32[]{:S(2)}) copy-start(f32[2]{0:T(128)S(1)} %slice_convert_fusion.5) | copy-start | bytes 28
  91.9 45.3 %copy-start.12 = (f32[2]{0:T(128)S(1)}, f32[2]{0:T(128)}, u32[]{:S(2)}) copy-start(f32[2]{0:T(128)} %copy-done.11) | copy-start | bytes 28
  98.6 40.2 %copy-start.4 = (bf16[4,128,2,64]{3,1,2,0:T(8,128)(2,1)S(1)}, bf16[4,128,2,64]{3,1,2,0:T(8,128)(2,1)}, u32[]{:S(2)}) copy-start(bf16[4,128,2,64]{3,1,2,0:T(8,128)(2,1)} %copy.59) | copy-start | bytes 393220
  98.6 40.2 %copy-start.5 = (bf16[4,128,2,64]{3,1,2,0:T(8,128)(2,1)S(1)}, bf16[4,128,2,64]{3,1,2,0:T(8,128)(2,1)}, u32[]{:S(2)}) copy-start(bf16[4,128,2,64]{3,1,2,0:T(8,128)(2,1)} %copy.60) | copy-start | bytes 393220
  110.7 29.4 %copy-start.18 = (f32[4,2,128]{2,1,0:T(2,128)S(1)}, f32[4,2,128]{2,1,0:T(2,128)}, u32[]{:S(2)}) copy-start(f32[4,2,128]{2,1,0:T(2,128)} %copy.63) | copy-start | bytes 12292
  142.9 8.0 %copy-start.23 = (f32[512]{0:T(512)S(1)}, f32[512]{0:T(512)}, u32[]{:S(2)}) copy-start(f32[512]{0:T(512)} %copy-done.22) | copy-start | bytes 6148
  142.9 8.0 %copy-start.26 = (f32[2048]{0:T(1024)S(1)}, f32[2048]{0:T(1024)}, u32[]{:S(2)}) copy-start(f32[2048]{0:T(1024)} %param.17) | copy-start | bytes 24580
  142.9 8.0 %copy-start.27 = (f32[256]{0:T(256)S(1)}, f32[256]{0:T(256)}, u32[]{:S(2)}) copy-start(f32[256]{0:T(256)} %param.22) | copy-start | bytes 3076
  158.4 18.6 %copy-start.3 = (bf16[384,2048]{1,0:T(8,128)(2,1)S(1)}, bf16[384,2048]{1,0:T(8,128)(2,1)}, u32[]{:S(2)}) copy-start(bf16[384,2048]{1,0:T(8,128)(2,1)} %reshape.379) | copy-start | bytes 4718596
  189.3 10.9 %copy-start.7 = (s32[256]{0:T(256)S(1)}, s32[256]{0:T(256)}, u32[]{:S(2)}) copy-start(s32[256]{0:T(256)} %copy-done.6) | copy-start | bytes 3076
  189.3 11.1 %copy-start.9 = (s32[128,2]{0,1:T(2,128)S(1)}, s32[128,2]{0,1:T(2,128)}, u32[]{:S(2)}) copy-start(s32[128,2]{0,1:T(2,128)} %param.27) | copy-start | bytes 3076
  189.3 11.3 %copy-start.19 = (f32[128,2]{0,1:T(2,128)S(1)}, f32[128,2]{0,1:T(2,128)}, u32[]{:S(2)}) copy-start(f32[128,2]{0,1:T(2,128)} %param.28) | copy-start | bytes 3076
  189.3 11.4 %copy-start.16 = (s32[256,1]{0,1:T(1,128)S(1)}, s32[256,1]{0,1:T(1,128)}, u32[]{:S(2)}) copy-start(s32[256,1]{0,1:T(1,128)} %copy-done.15) | copy-start | bytes 3076
  189.3 62.0 %all-to-all-start.1 = ((bf16[64,6,2048]{2,1,0:T(8,128)(2,1)}), bf16[64,6,2048]{2,1,0:T(8,128)(2,1)}, u32[]{:S(2)}, u32[]{:S(2)}) async-start(bf16[64,6,2048]{2,1,0:T(8,128)(2,1)} %reshape.380), calls=%async_computation.2 | async-start | bytes 4194304 | tf_op jit(solution)/shard_map/all_to_all | solution.py:190
  (3 other events, 2.0 us)
Sparse Core Ops, SparseCore 0:
  9.8 56.8 all-gather.9
  68.5 54.8 all-gather.11
  125.2 51.7 all-gather.13
  180.0 32.6 reduce-scatter.1
where the time goes:
time: 270 us; the launch traced here: 269 us
  blocking collectives  66.2 us (25%)
  waiting for transfers between devices  65.4 us (24%)
  local copies, waits for them, and re-layouts  41.3 us (15%)
  matrix products  35.1 us (13%)
  other arithmetic  23.3 us (9%)
  starting transfers between devices  23.1 us (9%)
  between operations  15 us (6%)
    all_gather x5, blocking collectives, carried_in(): lax.all_gather(part.astype(kind), axis)  63.8 us
    all_to_all x1, waiting for transfers between devices, expert_half(): lax.all_to_all(results, EP, split_axis=0, concat_axis=0, tiled=True)  50.6 us
    all_gather x1, waiting for transfers between devices, expert_half(): lax.all_gather(expert_down[0], 'tp', axis=0, tiled=True)  12.8 us
    all_to_all x1, starting transfers between devices, expert_half(): lax.all_to_all(outgoing, EP, split_axis=0, concat_axis=0, tiled=True)  12 us
    all_to_all x1, starting transfers between devices, expert_half(): lax.all_to_all(results, EP, split_axis=0, concat_axis=0, tiled=True)  10.9 us
    concatenate x8, local copies, waits for them, and re-layouts, rotate(): jnp.concatenate([first_half * cosine - second * sine_part, first_half * s...  10.8 us
    dot_general x3, matrix products, project(): jnp.dot(normed, weight, preferred_element_type=jnp.float32)  8.88 us
    dot_general x1, matrix products, expert_half(): jnp.dot(hidden, lax.all_gather(expert_down[0], 'tp', axis=0, tiled=True),...  8.59 us
  transfers between devices with their start and end apart: 6, of which 2 were waited for; matrix products, arithmetic and copies ran while one was open for 37% of the time, Pallas kernels for 0%

commit v1 on v0

--- a/solution.py
+++ b/solution.py
@@ -183,7 +183,9 @@
     hidden = (jax.nn.silu(gate_part) * up_part).astype(jnp.bfloat16)
     reduced = jnp.dot(
         hidden,
-        lax.all_gather(expert_down[0], "tp", axis=0, tiled=True),
+        jnp.concatenate(
+            lax.all_to_all(jnp.stack([expert_down[0]] * lax.axis_size("tp")), "tp", 0, 0), axis=0
+        ),
         preferred_element_type=jnp.float32,
     )
     results = reduced.astype(jnp.bfloat16).reshape(sources, capacity, width)

time: 270 us -> 285 us (1.056)
  blocking collectives: 66.2 us -> 87.4 us
  waiting for transfers between devices: 65.4 us -> 52 us
  other arithmetic: 23.3 us -> 26.9 us
    all_gather x5, blocking collectives: 63.8 us -> 84.9 us  [carried_in(): lax.all_gather(part.astype(kind), axis)]
    all_gather x1 -> x0, waiting for transfers between devices: 12.8 us -> none  [expert_half(): lax.all_gather(expert_down[0], 'tp', axis=0, tiled=True)]
    all_to_all x0 -> x1, starting transfers between devices: none -> 4.94 us  [expert_half(): lax.all_to_all(jnp.stack([expert_down[0]] * lax.axis_size('tp')), 'tp', 0...]
    concatenate x8, local copies, waits for them, and re-layouts: 10.8 us -> 5.89 us  [rotate(): jnp.concatenate([first_half * cosine - second * sine_part, first_half * s...]
    another operation x0 -> x1, local copies, waits for them, and re-layouts: none -> 3.69 us  [expert_half(): jnp.stack([expert_down[0]] * lax.axis_size('tp'))]
  transfers between devices with their start and end apart: 6 -> 6, of which waited for: 2 -> 1; matrix products, arithmetic and copies ran while one was open for 37% -> 36% of each run, Pallas kernels for 0% -> 0%
where the time goes in v1:
time: 285 us; the launch traced here: 283 us
  blocking collectives  87.4 us (31%)
  waiting for transfers between devices  52 us (18%)
  local copies, waits for them, and re-layouts  41.6 us (15%)
  matrix products  34.8 us (12%)
  other arithmetic  26.9 us (9%)
  starting transfers between devices  25.7 us (9%)
  between operations  15 us (5%)
    all_gather x5, blocking collectives, carried_in(): lax.all_gather(part.astype(kind), axis)  84.9 us
    all_to_all x1, waiting for transfers between devices, expert_half(): lax.all_to_all(results, EP, split_axis=0, concat_axis=0, tiled=True)  50.6 us
    all_to_all x1, starting transfers between devices, expert_half(): lax.all_to_all(outgoing, EP, split_axis=0, concat_axis=0, tiled=True)  12 us
    dot_general x3, matrix products, project(): jnp.dot(normed, weight, preferred_element_type=jnp.float32)  8.74 us
    all_to_all x1, starting transfers between devices, expert_half(): lax.all_to_all(results, EP, split_axis=0, concat_axis=0, tiled=True)  8.65 us
    dot_general x1, matrix products, expert_half(): jnp.dot(hidden, jnp.concatenate(lax.all_to_all(jnp.stack([expert_down[0]]...  8.58 us
    dot_general x1, matrix products, mixer_half(): jnp.dot(mixer_hidden, output_weight, preferred_element_type=jnp.float32)  6.01 us
    concatenate x8, local copies, waits for them, and re-layouts, rotate(): jnp.concatenate([first_half * cosine - second * sine_part, first_half * s...  5.89 us
  transfers between devices with their start and end apart: 6, of which 1 were waited for; matrix products, arithmetic and copies ran while one was open for 36% of the time, Pallas kernels for 0%

profile of v1, /device:TPU:2, one launch (start us, length us, event | category | flops | bytes accessed | tf_op | source)
XLA Modules:
  0.0 283.4 jit_solution(4708161926805726561)
XLA Ops:
  13.7 3.2 %gather_fusion = bf16[384,2048]{1,0:T(8,128)(2,1)} fusion(bf16[129,2048]{1,0:T(8,128)(2,1)S(1)} %concatenate.26, s32[1024]{0:T(1024)S(1)} %pad_clamp_fusion.1), kind=kCustom, calls=%fused_computation | custom fusion | bytes 3147264 | tf_op jit(solution)/shard_map/jit(_take)/gather | solution.py:176
  16.9 2.5 gather.13
  19.5 1.7 broadcast_select_fusion
  21.2 12.0 %all-to-all-start = ((bf16[64,6,2048]{2,1,0:T(8,128)(2,1)}), bf16[64,6,2048]{2,1,0:T(8,128)(2,1)S(1)}, u32[]{:S(2)}, u32[]{:S(2)}) async-start(bf16[64,6,2048]{2,1,0:T(8,128)(2,1)} %broadcast_select_fusion), calls=%async_computation.1 | async-start | bytes 4194304 | tf_op jit(solution)/shard_map/all_to_all | solution.py:177
  34.0 2.1 fusion
  38.0 2.4 all-reduce.1
  40.9 7.8 %all-gather.3 = bf16[4,1,2]{2,1,0:T(2,128)(2,1)S(1)} all-gather(bf16[1,1,2]{2,1,0:T(2,128)(2,1)S(1)} %convert_bitcast_fusion), channel_id=1, replica_groups=mesh['ep_0'=8,'ep_1'=4,'ep_2'=2,'tp'=4] {'ep_1'}, dimensions={0}, use_global_device_ids=true | all-gather | bytes 20 | tf_op jit(solution)/shard_map/all_gather | solution.py:25
  48.8 3.6 %convolution_convert_fusion.4 = bf16[512,256]{0,1:T(8,128)(2,1)} fusion(bf16[2048,256]{1,0:T(8,128)(2,1)} %param.18, bf16[512,2048]{1,0:T(8,128)(2,1)} %param.16, f32[2048]{0:T(1024)S(1)} %copy-done.27, f32[512]{0:T(512)S(1)} %add_rsqrt_fusion), kind=kOutput, calls=%fused_computation.26 | convolution fusion | flops 541196288 | bytes 3418112 | tf_op jit(solution)/shard_map/dot_general | solution.py:82
  52.5 1.7 convolution_convert_fusion.3
  54.7 37.2 %all-gather.4 = bf16[8,1,2]{2,1,0:T(2,128)(2,1)} all-gather(bf16[1,1,2]{2,1,0:T(2,128)(2,1)S(1)} %fusion.68), channel_id=1, replica_groups=mesh['ep_0'=8,'ep_1'=4,'ep_2'=2,'tp'=4] {'ep_0'}, dimensions={0}, use_global_device_ids=true | all-gather | bytes 36 | tf_op jit(solution)/shard_map/all_gather | solution.py:25
  100.3 3.4 %convolution_convert_fusion.5 = bf16[512,256]{1,0:T(8,128)(2,1)} fusion(bf16[2048,256]{1,0:T(8,128)(2,1)} %param.20, bf16[512,2048]{1,0:T(8,128)(2,1)} %param.16, f32[2048]{0:T(1024)} %param.17, f32[512]{0:T(512)} %copy-done.23), kind=kOutput, calls=%fused_computation.27 | convolution fusion | flops 541196288 | bytes 3418112 | tf_op jit(solution)/shard_map/dot_general | solution.py:82
  103.7 1.7 reshape.375
  111.0 1.9 all_gather.33
  118.1 3.7 %stack.5 = bf16[4,256,2048]{2,1,0:T(8,128)(2,1)} broadcast(bf16[256,2048]{1,0:T(8,128)(2,1)} %bitcast.149), dimensions={1,2} | broadcast | bytes 5242880 | tf_op jit(solution)/shard_map/stack | solution.py:187
  121.8 4.9 %all-to-all-start.1 = ((bf16[4,256,2048]{2,1,0:T(8,128)(2,1)}), bf16[4,256,2048]{2,1,0:T(8,128)(2,1)}, u32[]{:S(2)}, u32[]{:S(2)}) async-start(bf16[4,256,2048]{2,1,0:T(8,128)(2,1)} %stack.5), calls=%async_computation.2 | async-start | bytes 8388608 | tf_op jit(solution)/shard_map/all_to_all | solution.py:187
  126.9 12.6 %all_gather.34 = bf16[4,2,128,128]{3,2,1,0:T(8,128)(2,1)S(1)} all-gather(bf16[1,2,128,128]{3,2,1,0:T(8,128)(2,1)} %fusion.51), channel_id=1, replica_groups=mesh['ep_0'=8,'ep_1'=4,'ep_2'=2,'tp'=4] {'ep_1'}, dimensions={0}, use_global_device_ids=true | all-gather | bytes 327680 | tf_op jit(solution)/shard_map/all_gather | solution.py:25
  141.0 25.4 %all_gather.35 = bf16[8,2,128,128]{3,2,1,0:T(8,128)(2,1)S(1)} all-gather(bf16[1,2,128,128]{3,2,1,0:T(8,128)(2,1)S(1)} %fusion.50), channel_id=1, replica_groups=mesh['ep_0'=8,'ep_1'=4,'ep_2'=2,'tp'=4] {'ep_0'}, dimensions={0}, use_global_device_ids=true | all-gather | bytes 589824 | tf_op jit(solution)/shard_map/all_gather | solution.py:25
  166.4 1.5 multiply_add_fusion.1
  169.2 2.7 fusion.85
  171.9 2.1 copy.71
  177.5 2.3 sub.60
  179.9 6.0 %convolution_convert_fusion = bf16[512,2048]{1,0:T(8,128)(2,1)} fusion(bf16[256,2048]{1,0:T(8,128)(2,1)S(1)} %copy-done, f32[64,8,2,128]{3,2,1,0:T(2,128)} %bitcast.150, f32[64,8,2,128]{3,2,1,0:T(2,128)} %bitcast.151, f32[64,8,2,128]{3,2,1,0:T(2,128)} %bitcast.152, bf16[2048,256]{1,0:T(8,128)(2,1)} %param.21, f32[256]{0:T(256)S(1)} %copy-done.29, ...), kind=kOutput, calls=%fused_computation.12 | convolution fusion | flops 1080426496 | bytes 7875584 | tf_op jit(solution)/shard_map/dot_general | solution.py:144
  186.0 1.4 reshape.383
  187.4 5.7 %fusion.5 = f32[384,1024]{1,0:T(8,128)} fusion(bf16[384,2048]{1,0:T(8,128)(2,1)} %reshape.383, bf16[1,2048,1024]{2,1,0:T(8,128)(2,1)} %all-gather.8.cloned.1.call-done), kind=kOutput, calls=%fused_computation.10 | convolution fusion | flops 1610612736 | bytes 7340032 | tf_op jit(solution)/shard_map/dot_general | solution.py:181
  193.1 8.6 %convolution_convert_fusion.1 = bf16[384,2048]{1,0:T(8,128)(2,1)} fusion(bf16[1024,2048]{1,0:T(8,128)(2,1)} %bitcast.34, f32[384,1024]{1,0:T(8,128)} %fusion.5, bf16[384,2048]{1,0:T(8,128)(2,1)S(1)} %copy-done.4, bf16[1,2048,1024]{2,1,0:T(8,128)(2,1)} %all-gather.10.cloned.1.call-done), kind=kOutput, calls=%fused_computation.13 | convolution fusion | flops 3224371200 | bytes 13107200 | tf_op jit(solution)/shard_map/dot_general | solution.py:184
  201.7 3.7 %reshape.385 = bf16[64,6,2048]{2,1,0:T(8,128)(2,1)} reshape(bf16[384,2048]{1,0:T(8,128)(2,1)} %convolution_convert_fusion.1) | data formatting | bytes 3145728 | tf_op jit(solution)/shard_map/reshape | solution.py:191
  205.4 8.7 %all-to-all-start.2 = ((bf16[64,6,2048]{2,1,0:T(8,128)(2,1)}), bf16[64,6,2048]{2,1,0:T(8,128)(2,1)}, u32[]{:S(2)}, u32[]{:S(2)}) async-start(bf16[64,6,2048]{2,1,0:T(8,128)(2,1)} %reshape.385), calls=%async_computation.3 | async-start | bytes 4194304 | tf_op jit(solution)/shard_map/all_to_all | solution.py:192
  214.7 50.6 %all-to-all-done.2 = bf16[64,6,2048]{2,1,0:T(8,128)(2,1)} async-done(((bf16[64,6,2048]{2,1,0:T(8,128)(2,1)}), bf16[64,6,2048]{2,1,0:T(8,128)(2,1)}, u32[]{:S(2)}, u32[]{:S(2)}) %all-to-all-start.2) | async-done | bytes 1572896 | tf_op jit(solution)/shard_map/all_to_all | solution.py:192
  265.2 2.6 reshape.386
  267.8 2.3 gather_fusion.1
  270.2 1.7 gather.15
  271.9 4.9 %multiply_reduce_fusion = bf16[128,2048]{1,0:T(8,128)(2,1)} fusion(bf16[128,2,2048]{2,1,0:T(2,128)(2,1)S(1)} %gather.15, pred[128,2]{1,0:T(8,128)(4,1)S(1)} %copy.76, f32[128,2]{1,0:T(8,128)S(1)} %copy.78), kind=kLoop, calls=%fused_computation.14 | loop fusion | flops 1835008 | bytes 1574144 | tf_op jit(solution)/shard_map/reduce_sum | solution.py:196
  (148 shorter events, 35.6 us)
Async XLA Ops:
  7.2 172.7 %copy-start = (bf16[256,2048]{1,0:T(8,128)(2,1)S(1)}, bf16[256,2048]{1,0:T(8,128)(2,1)}, u32[]{:S(2)}) copy-start(bf16[256,2048]{1,0:T(8,128)(2,1)} %param.23) | copy-start | bytes 3145732
  7.2 4.1 %copy-start.3 = (bf16[128,2048]{1,0:T(8,128)(2,1)S(1)}, bf16[128,2048]{1,0:T(8,128)(2,1)}, u32[]{:S(2)}) copy-start(bf16[128,2048]{1,0:T(8,128)(2,1)} %param.25) | copy-start | bytes 1572868
  7.2 180.2 %all-gather.8.cloned.1.call-start = ((), (), s32[]{:S(2)}) async-start(), calls=%async_computation.5 | async-start | bytes 5242880 | tf_op jit(solution)/shard_map/all_gather | solution.py:180
  9.1 4.6 %copy-start.9 = (s32[256]{0:T(256)}, s32[256]{0:T(256)S(1)}, u32[]{:S(2)}) copy-start(s32[256]{0:T(256)S(1)} %convert_element_type.480) | copy-start | bytes 3076
  21.2 97.0 %all-to-all-start = ((bf16[64,6,2048]{2,1,0:T(8,128)(2,1)}), bf16[64,6,2048]{2,1,0:T(8,128)(2,1)S(1)}, u32[]{:S(2)}, u32[]{:S(2)}) async-start(bf16[64,6,2048]{2,1,0:T(8,128)(2,1)} %broadcast_select_fusion), calls=%async_computation.1 | async-start | bytes 4194304 | tf_op jit(solution)/shard_map/all_to_all | solution.py:177
  33.2 3.3 %copy-start.30 = (u32[256]{0:T(256)S(1)}, u32[256]{0:T(256)}, u32[]{:S(2)}) copy-start(u32[256]{0:T(256)} %constant.123) | copy-start | bytes 3076
  33.2 15.5 %copy-start.27 = (f32[2048]{0:T(1024)S(1)}, f32[2048]{0:T(1024)}, u32[]{:S(2)}) copy-start(f32[2048]{0:T(1024)} %param.17) | copy-start | bytes 24580
  33.2 159.9 %all-gather.10.cloned.1.call-start = ((), (), s32[]{:S(2)}) async-start(), calls=%async_computation.6 | async-start | bytes 5242880 | tf_op jit(solution)/shard_map/all_gather | solution.py:180
  36.1 16.3 %copy-start.23 = (f32[512]{0:T(512)}, f32[512]{0:T(512)S(1)}, u32[]{:S(2)}) copy-start(f32[512]{0:T(512)S(1)} %add_rsqrt_fusion) | copy-start | bytes 6148
  36.4 63.0 %copy-start.12 = (f32[4,2]{0,1:T(2,128)}, f32[4,2]{0,1:T(2,128)S(1)}, u32[]{:S(2)}) copy-start(f32[4,2]{0,1:T(2,128)S(1)} %get-tuple-element.2) | copy-start | bytes 100
  48.8 3.7 %copy-start.2 = (bf16[512,2048]{1,0:T(8,128)(2,1)S(1)}, bf16[512,2048]{1,0:T(8,128)(2,1)}, u32[]{:S(2)}) copy-start(bf16[512,2048]{1,0:T(8,128)(2,1)} %param.16) | copy-start | bytes 6291460
  48.8 3.7 %copy-start.26 = (bf16[2048,256]{1,0:T(8,128)(2,1)S(1)}, bf16[2048,256]{1,0:T(8,128)(2,1)}, u32[]{:S(2)}) copy-start(bf16[2048,256]{1,0:T(8,128)(2,1)} %param.19) | copy-start | bytes 3145732
  100.3 5.2 %copy-start.5 = (bf16[512,2,64]{0,2,1:T(8,128)(2,1)S(1)}, bf16[512,2,64]{0,2,1:T(8,128)(2,1)}, u32[]{:S(2)}) copy-start(bf16[512,2,64]{0,2,1:T(8,128)(2,1)} %get-tuple-element.14) | copy-start | bytes 393220
  108.1 9.3 %copy-start.13 = (f32[2]{0:T(128)}, f32[2]{0:T(128)S(1)}, u32[]{:S(2)}) copy-start(f32[2]{0:T(128)S(1)} %get-tuple-element.6) | copy-start | bytes 28
  108.1 9.3 %copy-start.14 = (f32[2]{0:T(128)}, f32[2]{0:T(128)S(1)}, u32[]{:S(2)}) copy-start(f32[2]{0:T(128)S(1)} %get-tuple-element.7) | copy-start | bytes 28
  110.9 6.5 %copy-start.1 = (f32[4,2,128,128]{3,2,1,0:T(8,128)}, f32[4,2,128,128]{3,2,1,0:T(8,128)S(1)}, u32[]{:S(2)}) copy-start(f32[4,2,128,128]{3,2,1,0:T(8,128)S(1)} %fusion.30) | copy-start | bytes 1572868
  117.4 4.4 %copy-start.15 = (f32[2]{0:T(128)}, f32[2]{0:T(128)S(1)}, u32[]{:S(2)}) copy-start(f32[2]{0:T(128)S(1)} %get-tuple-element.37) | copy-start | bytes 28
  121.8 71.3 %all-to-all-start.1 = ((bf16[4,256,2048]{2,1,0:T(8,128)(2,1)}), bf16[4,256,2048]{2,1,0:T(8,128)(2,1)}, u32[]{:S(2)}, u32[]{:S(2)}) async-start(bf16[4,256,2048]{2,1,0:T(8,128)(2,1)} %stack.5), calls=%async_computation.2 | async-start | bytes 8388608 | tf_op jit(solution)/shard_map/all_to_all | solution.py:187
  126.8 150.1 %reduce-scatter.2.cloned.1.call-start = ((), (), s32[]{:S(2)}) async-start(), calls=%async_computation.4 | async-start | bytes 2621440 | tf_op jit(solution)/shard_map/reduce_scatter | solution.py:143
  126.8 41.1 %copy-start.6 = (bf16[4,128,2,64]{3,1,2,0:T(8,128)(2,1)S(1)}, bf16[4,128,2,64]{3,1,2,0:T(8,128)(2,1)}, u32[]{:S(2)}) copy-start(bf16[4,128,2,64]{3,1,2,0:T(8,128)(2,1)} %copy.59) | copy-start | bytes 393220
  126.8 41.1 %copy-start.7 = (bf16[4,128,2,64]{3,1,2,0:T(8,128)(2,1)S(1)}, bf16[4,128,2,64]{3,1,2,0:T(8,128)(2,1)}, u32[]{:S(2)}) copy-start(bf16[4,128,2,64]{3,1,2,0:T(8,128)(2,1)} %copy.60) | copy-start | bytes 393220
  126.8 41.1 %copy-start.19 = (f32[4,128,2]{1,2,0:T(2,128)S(1)}, f32[4,128,2]{1,2,0:T(2,128)}, u32[]{:S(2)}) copy-start(f32[4,128,2]{1,2,0:T(2,128)} %copy.66) | copy-start | bytes 12292
  139.5 29.7 %copy-start.8 = (pred[128,128]{1,0:T(8,128)(4,1)S(1)}, pred[128,128]{1,0:T(8,128)(4,1)}, u32[]{:S(2)}) copy-start(pred[128,128]{1,0:T(8,128)(4,1)} %iota_compare_fusion.4) | copy-start | bytes 49156
  171.9 8.0 %copy-start.24 = (f32[512]{0:T(512)S(1)}, f32[512]{0:T(512)}, u32[]{:S(2)}) copy-start(f32[512]{0:T(512)} %copy-done.23) | copy-start | bytes 6148
  171.9 8.0 %copy-start.28 = (f32[2048]{0:T(1024)S(1)}, f32[2048]{0:T(1024)}, u32[]{:S(2)}) copy-start(f32[2048]{0:T(1024)} %param.17) | copy-start | bytes 24580
  171.9 8.0 %copy-start.29 = (f32[256]{0:T(256)S(1)}, f32[256]{0:T(256)}, u32[]{:S(2)}) copy-start(f32[256]{0:T(256)} %param.22) | copy-start | bytes 3076
  187.4 5.8 %copy-start.4 = (bf16[384,2048]{1,0:T(8,128)(2,1)S(1)}, bf16[384,2048]{1,0:T(8,128)(2,1)}, u32[]{:S(2)}) copy-start(bf16[384,2048]{1,0:T(8,128)(2,1)} %reshape.383) | copy-start | bytes 4718596
  205.4 8.7 %copy-start.10 = (s32[256]{0:T(256)S(1)}, s32[256]{0:T(256)}, u32[]{:S(2)}) copy-start(s32[256]{0:T(256)} %copy-done.9) | copy-start | bytes 3076
  205.4 8.9 %copy-start.11 = (s32[128,2]{0,1:T(2,128)S(1)}, s32[128,2]{0,1:T(2,128)}, u32[]{:S(2)}) copy-start(s32[128,2]{0,1:T(2,128)} %param.27) | copy-start | bytes 3076
  205.4 9.1 %copy-start.20 = (f32[128,2]{0,1:T(2,128)S(1)}, f32[128,2]{0,1:T(2,128)}, u32[]{:S(2)}) copy-start(f32[128,2]{0,1:T(2,128)} %param.28) | copy-start | bytes 3076
  205.4 9.2 %copy-start.17 = (s32[256,1]{0,1:T(1,128)S(1)}, s32[256,1]{0,1:T(1,128)}, u32[]{:S(2)}) copy-start(s32[256,1]{0,1:T(1,128)} %copy-done.16) | copy-start | bytes 3076
  205.4 59.8 %all-to-all-start.2 = ((bf16[64,6,2048]{2,1,0:T(8,128)(2,1)}), bf16[64,6,2048]{2,1,0:T(8,128)(2,1)}, u32[]{:S(2)}, u32[]{:S(2)}) async-start(bf16[64,6,2048]{2,1,0:T(8,128)(2,1)} %reshape.385), calls=%async_computation.3 | async-start | bytes 4194304 | tf_op jit(solution)/shard_map/all_to_all | solution.py:192
  (5 other events, 9.4 us)
Sparse Core Ops, SparseCore 0:
  9.8 56.8 all-gather.7
  68.5 54.8 all-gather.9
  186.1 32.0 reduce-scatter.1
